TPU v7x, 32 devices: a whole 2x2x4 slice. The times are simulated.
32 devices in a mesh: dp: 4 (over y, x), kv: 4 (over z), tp: 2 (over core).
Axes of the slice: x: 2, y: 2, z: 4, core: 2. Of those that a mesh axis runs over, the one named last changes fastest.
Arguments:
- tokens: bfloat16 [16, 2048], P('dp', 'kv'), may hold values from -700 to 700
- norm_gain: float32 [2048], P('kv'), may hold values from 0.1 to 1.9
- w_query: bfloat16 [2048, 2048], P('kv', 'tp'), may hold values from -0.25 to 0.25
- w_key: bfloat16 [2048, 2048], P('kv', 'tp'), may hold values from -0.125 to 0.125
- w_value: bfloat16 [2048, 2048], P('kv', 'tp'), may hold values from -0.125 to 0.125
- w_output: bfloat16 [2048, 2048], P('tp', 'kv'), may hold values from -0.125 to 0.125
- key_cache: bfloat16 [16, 2048, 16, 128], P('dp', 'kv', 'tp'), may hold values from -170 to 170
- value_cache: bfloat16 [16, 2048, 16, 128], P('dp', 'kv', 'tp'), may hold values from -6 to 6
- lengths: int32 [16], P('dp'), may hold values from 1024 to 2047, as said below
- lam: float32 [16], P('tp'), may hold values from 0.3 to 0.8
- head_gain: float32 [128], replicated, may hold values from 0.1 to 1.9
Outputs:
- attended: bfloat16 [16, 2048], P('dp', 'kv')
- new_key: bfloat16 [16, 2048], P('dp', 'tp')
- new_value: bfloat16 [16, 2048], P('dp', 'tp')
Inputs may be any that keep to these rules, and one draw needn't show every extreme that they name: `lengths`: exactly one sequence, chosen by the draw, has 2047 past tokens.
All inputs are finite; a program needn't handle non-finite values.
Results may differ from a plain program's by a relative error of at most 0.012.
Values may be sent and summed in bfloat16 or wider, within the bound.
A program may use at most 64 MiB of HBM per device.

v0:
```python
import jax
import jax.numpy as jnp
from jax import lax
from jax.sharding import PartitionSpec as P

D = 2048
HEAD_WIDTH = 64
VDIM = 128


epsilon = 1e-06


def joined(part, axis, combine):
    gathered = jax.tree.map(lambda a: lax.all_gather(a, axis), part)

    def take(source):
        return jax.tree.map(lambda a: lax.dynamic_index_in_dim(a, source, 0, False), gathered)

    return lax.fori_loop(
        1, lax.axis_size(axis), lambda source, state: combine(state, take(source)), take(0)
    )


def combine_parts(earlier, later):
    top = jnp.maximum(earlier[0], later[0])
    first = jnp.exp(earlier[0] - top)
    second = jnp.exp(later[0] - top)
    total = earlier[1] * first + later[1] * second
    summed = earlier[2] * first[..., None] + later[2] * second[..., None]
    return (top, total, summed)


def per_device(
    tokens,
    norm_gain,
    w_query,
    w_key,
    w_value,
    w_output,
    key_cache,
    value_cache,
    lengths,
    lam,
    head_gain,
):
    seqs = tokens.shape[0]
    heads_here = lam.shape[0]
    span = key_cache.shape[1]
    xfull = tokens.astype(jnp.float32)
    squares = jnp.sum(xfull * xfull, axis=-1)
    scaled = (xfull * norm_gain).astype(jnp.bfloat16)
    part_query = jnp.dot(scaled, w_query, preferred_element_type=jnp.float32)
    part_key = jnp.dot(scaled, w_key, preferred_element_type=jnp.float32)
    part_value = jnp.dot(scaled, w_value, preferred_element_type=jnp.float32)
    part_query, part_key, part_value, squares = lax.psum(
        (part_query, part_key, part_value, squares), "kv"
    )
    inv = lax.rsqrt(squares / D + epsilon)[:, None]
    query = (part_query * inv).astype(jnp.bfloat16)
    new_key = (part_key * inv).astype(jnp.bfloat16)
    new_value = (part_value * inv).astype(jnp.bfloat16)
    positions = lax.axis_index("kv") * span + jnp.arange(span, dtype=jnp.int32)
    hit = (positions[None, :] == lengths[:, None])[:, :, None, None]
    key_rows = jnp.where(hit, new_key.reshape(seqs, 1, heads_here, 2 * HEAD_WIDTH), key_cache)
    values = jnp.where(hit, new_value.reshape(seqs, 1, heads_here, VDIM), value_cache)
    logit_score = jnp.einsum(
        "bhmd,bphmd->bhmp",
        query.reshape(seqs, heads_here, 2, HEAD_WIDTH),
        key_rows.reshape(seqs, span, heads_here, 2, HEAD_WIDTH),
        preferred_element_type=jnp.float32,
    ) * HEAD_WIDTH ** (-0.5)
    live = (positions[None, :] <= lengths[:, None])[:, None, None, :]
    masked = jnp.where(live, logit_score, jnp.float32(-1e30))
    block_peak = jnp.max(masked, axis=-1)
    weights = jnp.where(live, jnp.exp(masked - block_peak[..., None]), jnp.float32(0.0))
    block_sum = jnp.sum(weights, axis=-1)
    acc = jnp.einsum(
        "bhmp,bphv->bhmv", weights.astype(jnp.bfloat16), values, preferred_element_type=jnp.float32
    )
    scale_lam = lam[None, :, None]
    top, total, summed = joined((block_peak, block_sum, acc), "kv", combine_parts)
    mixed = (
        summed[:, :, 0] / total[:, :, 0, None] - scale_lam * summed[:, :, 1] / total[:, :, 1, None]
    )
    normed = (
        mixed * lax.rsqrt(jnp.mean(mixed * mixed, axis=-1, keepdims=True) + epsilon) * head_gain
    )
    heads = normed.astype(jnp.bfloat16).reshape(seqs, heads_here * VDIM)
    partial_value = jnp.dot(heads, w_output, preferred_element_type=jnp.float32).astype(
        jnp.bfloat16
    )
    attended = lax.psum(partial_value, "tp").astype(jnp.float32).astype(jnp.bfloat16)
    return (attended, new_key, new_value)


def solution(mesh):
    in_specs = (
        P("dp", "kv"),
        P("kv"),
        P("kv", "tp"),
        P("kv", "tp"),
        P("kv", "tp"),
        P("tp", "kv"),
        P("dp", "kv", "tp", None),
        P("dp", "kv", "tp", None),
        P("dp"),
        P("tp"),
        P(),
    )
    out_specs = (P("dp", "kv"), P("dp", "tp"), P("dp", "tp"))
    return jax.shard_map(
        per_device, mesh=mesh, in_specs=in_specs, out_specs=out_specs, check_vma=False
    )
```

profile of v0, /device:TPU:0, one launch (start us, length us, event | category | flops | bytes accessed | tf_op | source)
XLA Modules:
  0.0 100.2 jit_solution(949048329724261872)
XLA Ops:
  0.6 0.0 copy-start
  0.6 1.2 %copy-done = bf16[512,1024]{1,0:T(8,128)(2,1)S(1)} copy-done((bf16[512,1024]{1,0:T(8,128)(2,1)S(1)}, bf16[512,1024]{1,0:T(8,128)(2,1)}, u32[]{:S(2)}) %copy-start) | copy-done | bytes 1048600
  1.9 0.9 fusion.23
  2.8 1.5 %fusion.25 = f32[4,1024]{1,0:T(4,128)S(1)} fusion(bf16[512,1024]{1,0:T(8,128)(2,1)} %param.16, bf16[4,512]{1,0:T(4,128)(2,1)} %param.13, f32[512]{0:T(512)} %param.14), kind=kOutput, calls=%fused_computation.60 | convolution fusion | flops 4200448 | bytes 1071104 | tf_op jit(solution)/shard_map/dot_general | solution.py:54
  4.3 1.5 %fusion.27 = f32[4,1024]{1,0:T(4,128)S(1)} fusion(bf16[512,1024]{1,0:T(8,128)(2,1)} %param.15, bf16[4,512]{1,0:T(4,128)(2,1)} %param.13, f32[512]{0:T(512)} %param.14), kind=kOutput, calls=%fused_computation.61 | convolution fusion | flops 4200448 | bytes 1071104 | tf_op jit(solution)/shard_map/dot_general | solution.py:53
  5.8 0.8 fusion.20
  6.6 21.5 %all-reduce = (f32[4,1024]{1,0:T(4,128)S(1)}, f32[4]{0:T(128)S(1)}, f32[4,1024]{1,0:T(4,128)S(1)}, f32[4,1024]{1,0:T(4,128)S(1)}) all-reduce(f32[4,1024]{1,0:T(4,128)S(1)} %fusion.27, f32[4]{0:T(128)S(1)} %fusion.20, f32[4,1024]{1,0:T(4,128)S(1)} %fusion.25, f32[4,1024]{1,0:T(4,128)S(1)} %fusion.23), channel_id=1, replica_groups=mesh['dp'=4,'kv'=4,'tp'=2] {'kv'}, use_global_device_ids=true, to_apply=%region_0.0 | all-reduce | flops 12292 | bytes 98336 | tf_op jit(solution)/shard_map/psum | solution.py:56
  28.2 0.1 multiply_convert_fusion
  28.3 0.0 copy-start.3
  28.3 0.0 copy-start.2
  28.3 0.7 broadcast_compare_fusion.1
  29.0 7.5 %copy.30 = bf16[4,512,8,128]{1,3,2,0:T(8,128)(2,1)} copy(bf16[4,512,8,128]{3,2,1,0:T(8,128)(2,1)} %param.19) | data formatting | bytes 8388608 | tf_op args[6]
  36.6 0.0 copy-done.3
  36.6 3.9 %broadcast_select_fusion = bf16[4,512,8,128]{1,3,2,0:T(8,128)(2,1)} fusion(bf16[4,512,8,128]{1,3,2,0:T(8,128)(2,1)} %copy.30, pred[4,512]{1,0:T(4,128)(4,1)S(1)} %get-tuple-element.225, bf16[4,8,128]{2,1,0:T(8,128)(2,1)S(1)} %bitcast.124), kind=kLoop, calls=%fused_computation.16 | loop fusion | flops 2097152 | bytes 8398848 | tf_op jit(solution)/shard_map/jit(_where)/select_n | solution.py:65
  40.4 0.1 reshape.106
  40.5 2.8 %fusion.31 = f32[4,8,2,1,512]{4,3,2,1,0:T(1,128)S(1)} fusion(bf16[4,8,2,64,1]{3,4,2,1,0:T(2,128)(2,1)S(1)} %reshape.106, bf16[4,512,8,2,64]{1,4,3,2,0:T(8,128)(2,1)} %bitcast.116), kind=kOutput, calls=%fused_computation.64 | convolution fusion | flops 4194304 | bytes 4333568 | tf_op jit(solution)/shard_map/bhmd,bphmd->bhmp/dot_general | solution.py:67
  43.4 0.2 fusion.11
  43.5 0.0 copy-done.2
  43.6 7.5 %copy.33 = bf16[4,512,8,128]{1,3,2,0:T(8,128)(2,1)} copy(bf16[4,512,8,128]{3,2,1,0:T(8,128)(2,1)} %param.20) | data formatting | bytes 8388608 | tf_op args[7]
  51.1 0.0 copy-start.4
  51.1 0.0 copy-start.5
  51.1 0.0 copy-start.1
  51.1 3.5 %fusion.5 = f32[4,8,2,128]{3,2,1,0:T(2,128)S(1)} fusion(bf16[4,512,8,128]{1,3,2,0:T(8,128)(2,1)} %copy.33, pred[4,512]{1,0:T(4,128)(4,1)S(1)} %get-tuple-element.225, bf16[4,8,128]{2,1,0:T(8,128)(2,1)S(1)} %bitcast.125, pred[4,512]{1,0:T(4,128)(4,1)S(1)} %get-tuple-element.224, f32[4,8,2]{2,1,0:T(8,128)S(1)} %fusion.11, f32[4,8,2,1,512]{4,3,2,1,0:T(1,128)S(1)} %fusion.31), kind=kOutput, calls=%fused_computation.13 | convolution fusion | flops 10649600 | bytes 4370688 | tf_op jit(solution)/shard_map/bhmp,bphv->bhmv/dot_general | solution.py:78
  54.6 13.4 %all-gather.2 = f32[16,8,2,128]{3,1,2,0:T(8,128)S(1)} all-gather(f32[4,8,2,128]{3,1,2,0:T(8,128)S(1)} %copy.35), channel_id=4, replica_groups=mesh['dp'=4,'kv'=4,'tp'=2] {'kv'}, dimensions={0}, use_global_device_ids=true | all-gather | bytes 163840 | tf_op jit(solution)/shard_map/all_gather | solution.py:15
  68.1 0.3 fusion.29
  68.4 0.1 copy.32
  68.5 13.2 %all-gather.1 = f32[16,8,2]{1,2,0:T(2,128)S(1)} all-gather(f32[4,8,2]{1,2,0:T(2,128)S(1)} %copy.32), channel_id=3, replica_groups=mesh['dp'=4,'kv'=4,'tp'=2] {'kv'}, dimensions={0}, use_global_device_ids=true | all-gather | bytes 1280 | tf_op jit(solution)/shard_map/all_gather | solution.py:15
  81.7 0.1 copy.31
  81.8 13.2 %all-gather = f32[16,8,2]{1,2,0:T(2,128)S(1)} all-gather(f32[4,8,2]{1,2,0:T(2,128)S(1)} %copy.31), channel_id=2, replica_groups=mesh['dp'=4,'kv'=4,'tp'=2] {'kv'}, dimensions={0}, use_global_device_ids=true | all-gather | bytes 1280 | tf_op jit(solution)/shard_map/all_gather | solution.py:15
  95.0 1.5 %while.19 = (s32[]{:T(128)}, f32[4,8,2]{1,0,2:T(4,128)S(1)}, f32[4,8,2]{1,0,2:T(4,128)S(1)}, f32[4,8,2,128]{3,2,1,0:T(2,128)S(1)}, f32[4,4,8,2]{2,3,1,0:T(2,128)...) while((s32[]{:T(128)}, f32[4,8,2]{1,0,2:T(4,128)S(1)}, ...), condition=%wide.region_8.9_spmd, body=%wide.region_7.8_spmd.sunk | while | flops 24965 | bytes 168599 | solution.py:20
  95.0 0.1 copy.117
  95.1 0.1 copy.118
  95.2 0.2 fusion.41
  95.5 0.1 copy.117
  95.6 0.1 copy.118
  95.7 0.2 fusion.41
  96.0 0.1 copy.117
  96.1 0.1 copy.118
  96.2 0.2 fusion.41
  96.5 0.1 slice_reduce_fusion
  96.5 0.0 copy-done.4
  96.6 0.2 broadcast_bitcast_fusion.2
  96.7 0.1 broadcast_bitcast_fusion
  96.8 0.0 copy-done.5
  96.8 0.1 broadcast_bitcast_fusion.3
  96.9 0.0 copy-done.1
  96.9 0.2 convolution_convert_fusion
  97.1 3.0 %psum.39 = bf16[4,512]{1,0:T(4,128)(2,1)} all-reduce(bf16[4,512]{1,0:T(4,128)(2,1)S(1)} %convolution_convert_fusion), channel_id=1, replica_groups=mesh['dp'=4,'kv'=4,'tp'=2] {'tp'}, use_global_device_ids=true, to_apply=%region_10.11 | all-reduce | flops 2048 | bytes 8192 | tf_op jit(solution)/shard_map/psum | solution.py:93
  (24 shorter events, 0.2 us)
Async XLA Ops:
  0.6 1.2 %copy-start = (bf16[512,1024]{1,0:T(8,128)(2,1)S(1)}, bf16[512,1024]{1,0:T(8,128)(2,1)}, u32[]{:S(2)}) copy-start(bf16[512,1024]{1,0:T(8,128)(2,1)} %param.17) | copy-start | bytes 3145732
  28.3 8.3 %copy-start.3 = (bf16[4,1024]{1,0:T(4,128)(2,1)}, bf16[4,1024]{1,0:T(4,128)(2,1)S(1)}, u32[]{:S(2)}) copy-start(bf16[4,1024]{1,0:T(4,128)(2,1)S(1)} %get-tuple-element.230) | copy-start | bytes 24580
  28.3 15.3 %copy-start.2 = (bf16[4,1024]{1,0:T(4,128)(2,1)}, bf16[4,1024]{1,0:T(4,128)(2,1)S(1)}, u32[]{:S(2)}) copy-start(bf16[4,1024]{1,0:T(4,128)(2,1)S(1)} %get-tuple-element.229) | copy-start | bytes 24580
  51.1 45.4 %copy-start.4 = (f32[8]{0:T(128)S(1)}, f32[8]{0:T(128)}, u32[]{:S(2)}) copy-start(f32[8]{0:T(128)} %param.22) | copy-start | bytes 100
  51.1 45.7 %copy-start.5 = (f32[128]{0:T(128)S(1)}, f32[128]{0:T(128)}, u32[]{:S(2)}) copy-start(f32[128]{0:T(128)} %param.23) | copy-start | bytes 1540
  51.1 45.8 %copy-start.1 = (bf16[1024,512]{1,0:T(8,128)(2,1)S(1)}, bf16[1024,512]{1,0:T(8,128)(2,1)}, u32[]{:S(2)}) copy-start(bf16[1024,512]{1,0:T(8,128)(2,1)} %param.18) | copy-start | bytes 3145732
where the time goes:
time: 101 us; the launch traced here: 100 us
  blocking collectives  64.4 us (64%)
  local copies, waits for them, and re-layouts  17.5 us (17%)
  matrix products  10.6 us (10%)
  other arithmetic  6.88 us (7%)
    all_gather x3, blocking collectives, joined(): gathered = jax.tree.map(lambda a: lax.all_gather(a, axis), part)  39.8 us
    psum x1, blocking collectives, per_device(): lax.psum((part_query, part_key, part_value, squares), 'kv')  21.5 us
    unnamed x18, local copies, waits for them, and re-layouts  16.4 us
    select_n x1, other arithmetic, per_device(): jnp.where(hit, new_key.reshape(seqs, 1, heads_here, 2 * HEAD_WIDTH), key_...  3.86 us
    dot_general x1, matrix products, per_device(): jnp.einsum('bhmp,bphv->bhmv', weights.astype(jnp.bfloat16), values, prefe...  3.53 us
    psum x1, blocking collectives, per_device(): lax.psum(partial_value, 'tp').astype(jnp.float32).astype(jnp.bfloat16)  3.05 us
    dot_general x1, matrix products, per_device(): jnp.einsum('bhmd,bphmd->bhmp', query.reshape(seqs, heads_here, 2, HEAD_WI...  2.83 us

commit v1 on v0

v1 whole, which is shorter than its diff:
```python
import functools

import jax
import jax.numpy as jnp
from jax import lax
from jax.experimental import pallas as pl
from jax.experimental.pallas import tpu as pltpu
from jax.sharding import PartitionSpec as P

MESH = pl.DeviceIdType.MESH
epsilon = 1e-06
HBM = pl.ANY


def kernel(
    n, ntp, d_model, head_width,
    x_hbm, g_hbm, wq_hbm, wk_hbm, wv_hbm, wo_hbm, kc_hbm, vc_hbm, len_hbm, lam_hbm, hg_hbm,
    out_ref, nk_ref, nv_ref,
    x_s, g_s, wq_s, wk_s, wv_s, wo_s, kc_s, vc_s, len_s, lam_s, hg_s,
    q_all, kv_all, acc_all, stat_all, tp_all, bias_s, q_rows, k_rows, v_rows, head_rows,
    load_sem, k_sem, v_sem,
    q_send, q_recv, kv_send, kv_recv, acc_send, acc_recv, stat_send, stat_recv, tp_send, tp_recv,
):
    me = lax.axis_index("kv")
    side = lax.axis_index("tp")
    seqs = x_s.shape[0]
    width = wq_s.shape[1]
    vdim = hg_s.shape[1]
    heads = width // vdim
    cols = kc_s.shape[1]
    span = cols // heads
    f32 = jnp.float32

    def load(src, dst, i):
        copy = pltpu.make_async_copy(src, dst, load_sem.at[i])
        copy.start()
        return copy

    x_load = load(x_hbm, x_s, 0)
    g_load = load(g_hbm, g_s, 1)
    wq_load = load(wq_hbm, wq_s, 2)
    len_load = load(len_hbm, len_s, 3)
    wk_load = load(wk_hbm, wk_s, 4)
    wv_load = load(wv_hbm, wv_s, 5)
    lam_load = load(lam_hbm, lam_s, 6)
    hg_load = load(hg_hbm, hg_s, 7)

    barrier = pltpu.get_barrier_semaphore()
    for o in range(1, n):
        pl.semaphore_signal(
            barrier, inc=1, device_id={"kv": lax.rem(me + o, n)}, device_id_type=MESH
        )
    for o in range(1, ntp):
        pl.semaphore_signal(
            barrier, inc=1, device_id={"tp": lax.rem(side + o, ntp)}, device_id_type=MESH
        )

    def send_kv(buf, at, send, recv):
        for o in range(1, n):
            pltpu.make_async_remote_copy(
                src_ref=buf.at[at(me)], dst_ref=buf.at[at(me)],
                send_sem=send(o), recv_sem=recv(me),
                device_id={"kv": lax.rem(me + o, n)}, device_id_type=MESH,
            ).start()

    def wait_kv(buf, at, send, recv, sent):
        for o in range(1, n):
            src = lax.rem(me + o, n)
            copy = pltpu.make_async_remote_copy(
                src_ref=buf.at[at(src)], dst_ref=buf.at[at(src)],
                send_sem=send(o), recv_sem=recv(src),
                device_id={"kv": src}, device_id_type=MESH,
            )
            if sent:
                copy.wait_send()
            else:
                copy.wait_recv()

    x_load.wait()
    g_load.wait()
    xf = x_s[...].astype(f32)
    squares = jnp.sum(xf * xf, axis=-1, keepdims=True)
    scaled = (xf * g_s[...]).astype(jnp.bfloat16)
    wq_load.wait()
    k_loads, v_loads = [], []
    for b in range(seqs):
        copy = pltpu.make_async_copy(kc_hbm.at[b], kc_s.at[b], k_sem.at[b])
        copy.start()
        k_loads.append(copy)
    for b in range(seqs):
        copy = pltpu.make_async_copy(vc_hbm.at[b], vc_s.at[b], v_sem.at[b])
        copy.start()
        v_loads.append(copy)
    wo_load = load(wo_hbm, wo_s, 8)

    q_all[me, :, :width] = jnp.dot(scaled, wq_s[...], preferred_element_type=f32)
    q_all[me, :, width:] = jnp.broadcast_to(squares, (seqs, q_all.shape[2] - width))
    pl.semaphore_wait(barrier, n - 1 + ntp - 1)
    whole = lambda s: s
    q_args = (q_all, whole, lambda o: q_send.at[o], lambda s: q_recv.at[s])
    kv_args = (kv_all, whole, lambda o: kv_send.at[o], lambda s: kv_recv.at[s])
    stat_args = (stat_all, whole, lambda o: stat_send.at[o], lambda s: stat_recv.at[s])
    acc_args = [
        (
            acc_all,
            lambda s, b=b: (s, b),
            lambda o, b=b: acc_send.at[o, b],
            lambda s, b=b: acc_recv.at[s, b],
        )
        for b in range(seqs)
    ]
    send_kv(*q_args)
    wk_load.wait()
    kv_all[me, :, :width] = jnp.dot(scaled, wk_s[...], preferred_element_type=f32)
    wv_load.wait()
    kv_all[me, :, width:] = jnp.dot(scaled, wv_s[...], preferred_element_type=f32)
    send_kv(*kv_args)

    len_load.wait()
    lam_load.wait()
    hg_load.wait()
    col = lax.broadcasted_iota(jnp.int32, (2 * heads, cols), 1)
    row = lax.broadcasted_iota(jnp.int32, (2 * heads, cols), 0)
    diagonal = lax.rem(col, heads) == lax.rem(row, heads)
    local = [len_s[b] - me * span for b in range(seqs)]
    for b in range(seqs):
        bias_s[b] = jnp.where(diagonal & (col < local[b] * heads), f32(0.0), f32(-jnp.inf))
    lane = lax.broadcasted_iota(jnp.int32, (2 * heads, vdim), 1)
    half = lax.broadcasted_iota(jnp.int32, (2 * heads, vdim), 0) // heads
    own_map = (lane // head_width) == half

    wait_kv(*q_args, False)
    total = q_all[0]
    for s in range(1, n):
        total = total + q_all[s]
    inv = lax.rsqrt(total[:, width : width + 1] / d_model + epsilon)
    query = (total[:, :width] * inv).astype(jnp.bfloat16).astype(f32)
    for h in range(heads):
        q_rows[:, h, :] = query[:, h * vdim : (h + 1) * vdim]

    def doubled(rows):
        return jnp.concatenate([rows, rows], axis=0)

    queries, scores = [], []
    for b in range(seqs):
        q_b = jnp.where(own_map, doubled(q_rows[b]), f32(0.0))
        queries.append(q_b)
    for b in range(seqs):
        k_loads[b].wait()
        scores.append(
            lax.dot_general(
                (queries[b] * head_width**-0.5).astype(jnp.bfloat16), kc_s[b],
                (((1,), (1,)), ((), ())), preferred_element_type=f32,
            )
            + bias_s[b]
        )
        bias_s[b] = scores[b]

    wait_kv(*kv_args, False)
    total = kv_all[0]
    for s in range(1, n):
        total = total + kv_all[s]
    fresh = (total * inv).astype(jnp.bfloat16)
    nk_ref[...] = fresh[:, :width]
    nv_ref[...] = fresh[:, width:]
    fresh = fresh.astype(f32)
    for h in range(heads):
        k_rows[:, h, :] = fresh[:, h * vdim : (h + 1) * vdim]
        v_rows[:, h, :] = fresh[:, width + h * vdim : width + (h + 1) * vdim]

    stats = jnp.zeros((2 * heads, stat_all.shape[2]), f32)
    stat_lane = lax.broadcasted_iota(jnp.int32, stats.shape, 1)
    for b in range(seqs):
        new_score = jnp.sum(queries[b] * doubled(k_rows[b]), axis=-1, keepdims=True)
        here = (local[b] >= 0) & (local[b] < span)
        new_score = jnp.where(here, new_score * head_width**-0.5, f32(-jnp.inf))
        score = bias_s[b]
        peak = jnp.maximum(jnp.max(score, axis=-1, keepdims=True), new_score)
        peak = jnp.maximum(peak, f32(-1e30))
        weights = jnp.exp(score - peak)
        new_weight = jnp.exp(new_score - peak)
        block_sum = jnp.sum(weights, axis=-1, keepdims=True) + new_weight
        v_loads[b].wait()
        acc = jnp.dot(weights.astype(jnp.bfloat16), vc_s[b], preferred_element_type=f32)
        acc_all[me, b] = acc + new_weight.astype(jnp.bfloat16).astype(f32) * doubled(v_rows[b])
        send_kv(*acc_args[b])
        stats = jnp.where(stat_lane == b, peak, stats)
        stats = jnp.where(stat_lane == seqs + b, block_sum, stats)
    stat_all[me] = stats
    send_kv(*stat_args)

    h_row = lax.broadcasted_iota(jnp.int32, (heads, 1), 0)
    lam = jnp.zeros((heads, 1), f32)
    for h in range(heads):
        lam = jnp.where(h_row == h, lam_s[h], lam)

    wait_kv(*stat_args, False)
    for b in range(seqs):
        peaks = [stat_all[s][:, b : b + 1] for s in range(n)]
        sums = [stat_all[s][:, seqs + b : seqs + b + 1] for s in range(n)]
        top = functools.reduce(jnp.maximum, peaks)
        factors = [jnp.exp(p - top) for p in peaks]
        whole_sum = sum(l * f for l, f in zip(sums, factors))
        wait_kv(*acc_args[b], False)
        summed = acc_all[0, b] * factors[0]
        for s in range(1, n):
            summed = summed + acc_all[s, b] * factors[s]
        maps = summed / whole_sum
        mixed = maps[:heads] - lam * maps[heads:]
        normed = (
            mixed
            * lax.rsqrt(jnp.mean(mixed * mixed, axis=-1, keepdims=True) + epsilon)
            * hg_s[...]
        )
        head_rows[b] = normed
    flat = jnp.concatenate(
        [head_rows[:, h, :].astype(jnp.bfloat16) for h in range(heads)], axis=-1
    )
    wo_load.wait()
    tp_all[side] = jnp.dot(flat, wo_s[...], preferred_element_type=f32).astype(jnp.bfloat16)
    for o in range(1, ntp):
        pltpu.make_async_remote_copy(
            src_ref=tp_all.at[side], dst_ref=tp_all.at[side],
            send_sem=tp_send.at[o], recv_sem=tp_recv.at[side],
            device_id={"tp": lax.rem(side + o, ntp)}, device_id_type=MESH,
        ).start()
    wait_kv(*q_args, True)
    wait_kv(*kv_args, True)
    wait_kv(*stat_args, True)
    for b in range(seqs):
        wait_kv(*acc_args[b], True)
    for o in range(1, ntp):
        src = lax.rem(side + o, ntp)
        copy = pltpu.make_async_remote_copy(
            src_ref=tp_all.at[src], dst_ref=tp_all.at[src],
            send_sem=tp_send.at[o], recv_sem=tp_recv.at[src],
            device_id={"tp": src}, device_id_type=MESH,
        )
        copy.wait_recv()
        copy.wait_send()
    result = tp_all[0].astype(f32)
    for s in range(1, ntp):
        result = result + tp_all[s].astype(f32)
    out_ref[...] = result.astype(jnp.bfloat16)


def per_device(
    n, ntp,
    tokens, norm_gain, w_query, w_key, w_value, w_output,
    key_cache, value_cache, lengths, lam, head_gain,
):
    seqs, features = tokens.shape
    width = w_query.shape[1]
    heads = lam.shape[0]
    vdim = head_gain.shape[0]
    span = key_cache.shape[1]
    columns = w_output.shape[1]
    bf16, f32 = jnp.bfloat16, jnp.float32
    vmem, dma = pltpu.VMEM, pltpu.SemaphoreType.DMA
    keys = key_cache.reshape(seqs, span * heads, vdim)
    values = value_cache.reshape(seqs, span * heads, vdim)
    body = functools.partial(kernel, n, ntp, features * n, vdim // 2)
    return pl.pallas_call(
        body,
        out_shape=(
            jax.ShapeDtypeStruct((seqs, columns), bf16),
            jax.ShapeDtypeStruct((seqs, width), bf16),
            jax.ShapeDtypeStruct((seqs, width), bf16),
        ),
        in_specs=[pl.BlockSpec(memory_space=HBM)] * 11,
        out_specs=(pl.BlockSpec(memory_space=pltpu.VMEM),) * 3,
        scratch_shapes=[
            vmem((seqs, features), bf16),
            vmem((1, features), f32),
            vmem(w_query.shape, bf16),
            vmem(w_key.shape, bf16),
            vmem(w_value.shape, bf16),
            vmem(w_output.shape, bf16),
            vmem(keys.shape, bf16),
            vmem(values.shape, bf16),
            pltpu.SMEM((seqs,), jnp.int32),
            pltpu.SMEM((heads,), f32),
            vmem((1, vdim), f32),
            vmem((n, seqs, width + 128), f32),
            vmem((n, seqs, 2 * width), f32),
            vmem((n, seqs, 2 * heads, vdim), f32),
            vmem((n, 2 * heads, 128), f32),
            vmem((ntp, seqs, columns), bf16),
            vmem((seqs, 2 * heads, span * heads), f32),
            vmem((seqs, heads, vdim), f32),
            vmem((seqs, heads, vdim), f32),
            vmem((seqs, heads, vdim), f32),
            vmem((seqs, heads, vdim), f32),
            dma((9,)), dma((seqs,)), dma((seqs,)),
            dma((n,)), dma((n,)), dma((n,)), dma((n,)),
            dma((n, seqs)), dma((n, seqs)), dma((n,)), dma((n,)),
            dma((ntp,)), dma((ntp,)),
        ],
        compiler_params=pltpu.CompilerParams(
            collective_id=0, has_side_effects=True, vmem_limit_bytes=56 * 1024 * 1024
        ),
    )(
        tokens, norm_gain.reshape(1, -1), w_query, w_key, w_value, w_output,
        keys, values, lengths, lam, head_gain.reshape(1, -1),
    )


def solution(mesh):
    in_specs = (
        P("dp", "kv"),
        P("kv"),
        P("kv", "tp"),
        P("kv", "tp"),
        P("kv", "tp"),
        P("tp", "kv"),
        P("dp", "kv", "tp", None),
        P("dp", "kv", "tp", None),
        P("dp"),
        P("tp"),
        P(),
    )
    out_specs = (P("dp", "kv"), P("dp", "tp"), P("dp", "tp"))
    return jax.shard_map(
        functools.partial(per_device, mesh.shape["kv"], mesh.shape["tp"]),
        mesh=mesh, in_specs=in_specs, out_specs=out_specs, check_vma=False,
    )
```

time: 101 us -> 25.1 us (0.25)
  blocking collectives: 64.4 us -> 0 us
  Pallas kernels: 0 us -> 20.2 us
  local copies, waits for them, and re-layouts: 17.5 us -> 3.87 us
  matrix products: 10.6 us -> 0 us
  other arithmetic: 6.88 us -> 0 us
    all_gather x3 -> x0, blocking collectives: 39.8 us -> none  [joined(): gathered = jax.tree.map(lambda a: lax.all_gather(a, axis), part)]
    psum x2 -> x0, blocking collectives: 24.6 us -> none  [the longest x1 21.5 us: per_device(): lax.psum((part_query, part_key, part_value, squares), 'kv')]
    pallas_call x0 -> x1, Pallas kernels: none -> 20.2 us  [per_device(): pl.pallas_call(body, out_shape=(jax.ShapeDtypeStruct((seqs, columns), bf1...]
    unnamed x18 -> x3, local copies, waits for them, and re-layouts: 16.4 us -> 3.87 us
    dot_general x6 -> x0, matrix products: 10.6 us -> none  [the longest x1 3.53 us: per_device(): jnp.einsum('bhmp,bphv->bhmv', weights.astype(jnp.bfloat16), values, prefe...]
    select_n x1 -> x0, other arithmetic: 3.86 us -> none  [per_device(): jnp.where(hit, new_key.reshape(seqs, 1, heads_here, 2 * HEAD_WIDTH), key_...]
    reduce_sum x2 -> x0, other arithmetic: 1.07 us -> none  [the longest x1 0.81 us: per_device(): squares = jnp.sum(xfull * xfull, axis=-1)]
where the time goes in v1:
time: 25.1 us; the launch traced here: 24.8 us
  Pallas kernels  20.2 us (80%)
  local copies, waits for them, and re-layouts  3.87 us (15%)
  between operations  0.64 us (3%)
    pallas_call x1, Pallas kernels, per_device(): pl.pallas_call(body, out_shape=(jax.ShapeDtypeStruct((seqs, columns), bf1...  20.2 us
    unnamed x3, local copies, waits for them, and re-layouts  3.87 us

profile of v1, /device:TPU:0, one launch (start us, length us, event | category | flops | bytes accessed | tf_op | source)
XLA Modules:
  0.0 24.8 jit_solution(1808432397400541532)
XLA Ops:
  0.6 20.2 %shard_map.130 = (bf16[4,512]{1,0:T(4,128)(2,1)}, bf16[4,1024]{1,0:T(4,128)(2,1)}, bf16[4,1024]{1,0:T(4,128)(2,1)}) custom-call(bf16[4,512]{1,0:T(4,128)(2,1)} %x_hbm.1, f32[1,512]{1,0:T(1,128)} %bitcast.6, bf16[512,1024]{1,0:T(8,128)(2,1)} %wq_hbm.1, bf16[512,1024]{1,0:T(8,128)(2,1)} %wk_hbm.1, bf16[512,1024]{1,0:T(8,128)(2,1)} %wv_hbm.1, ...), custom_call_target="tpu_custom_call" | custom-call | tf_op jit(solution)/shard_map/pallas_call | solution.py:263
  20.9 1.3 %copy.17 = bf16[4,512]{1,0:T(4,128)(2,1)} copy(bf16[4,512]{1,0:T(4,128)(2,1)} %get-tuple-element.6) | data formatting | bytes 8192
  22.2 1.3 %copy.18 = bf16[4,1024]{1,0:T(4,128)(2,1)} copy(bf16[4,1024]{1,0:T(4,128)(2,1)} %get-tuple-element.7) | data formatting | bytes 16384
  23.5 1.3 %copy.19 = bf16[4,1024]{1,0:T(4,128)(2,1)} copy(bf16[4,1024]{1,0:T(4,128)(2,1)} %get-tuple-element.8) | data formatting | bytes 16384

commit v2 on v1

--- a/solution.py
+++ b/solution.py
@@ -9,7 +9,7 @@
 
 MESH = pl.DeviceIdType.MESH
 epsilon = 1e-06
-HBM = pl.ANY
+HBM = pltpu.HBM
 
 
 def kernel(
@@ -17,9 +17,9 @@
     x_hbm, g_hbm, wq_hbm, wk_hbm, wv_hbm, wo_hbm, kc_hbm, vc_hbm, len_hbm, lam_hbm, hg_hbm,
     out_ref, nk_ref, nv_ref,
     x_s, g_s, wq_s, wk_s, wv_s, wo_s, kc_s, vc_s, len_s, lam_s, hg_s,
-    q_all, kv_all, acc_all, stat_all, tp_all, bias_s, q_rows, k_rows, v_rows, head_rows,
+    q_all, kv_part, kv_in, kv_out, acc_all, stat_all, tp_all, bias_s, q_rows, fresh_s, head_rows,
     load_sem, k_sem, v_sem,
-    q_send, q_recv, kv_send, kv_recv, acc_send, acc_recv, stat_send, stat_recv, tp_send, tp_recv,
+    q_send, q_recv, part_send, part_recv, kv_send, kv_recv, acc_send, acc_recv, stat_send, stat_recv, tp_send, tp_recv,
 ):
     me = lax.axis_index("kv")
     side = lax.axis_index("tp")
@@ -63,8 +63,8 @@
                 device_id={"kv": lax.rem(me + o, n)}, device_id_type=MESH,
             ).start()
 
-    def wait_kv(buf, at, send, recv, sent):
-        for o in range(1, n):
+    def wait_kv(buf, at, send, recv, sent, offsets=range(1, n)):
+        for o in offsets:
             src = lax.rem(me + o, n)
             copy = pltpu.make_async_remote_copy(
                 src_ref=buf.at[at(src)], dst_ref=buf.at[at(src)],
@@ -98,7 +98,7 @@
     pl.semaphore_wait(barrier, n - 1 + ntp - 1)
     whole = lambda s: s
     q_args = (q_all, whole, lambda o: q_send.at[o], lambda s: q_recv.at[s])
-    kv_args = (kv_all, whole, lambda o: kv_send.at[o], lambda s: kv_recv.at[s])
+    kv_args = (kv_out, whole, lambda o: kv_send.at[o], lambda s: kv_recv.at[s])
     stat_args = (stat_all, whole, lambda o: stat_send.at[o], lambda s: stat_recv.at[s])
     acc_args = [
         (
@@ -110,11 +110,20 @@
         for b in range(seqs)
     ]
     send_kv(*q_args)
+    units = kv_part.shape[1]
+
+    def keep_part(part, first):
+        for h in range(heads):
+            slab = part[:, h * vdim : (h + 1) * vdim]
+            at = (first + h) * seqs
+            step = min(seqs, units)
+            for r in range(0, seqs, step):
+                kv_part[(at + r) // units, pl.ds((at + r) % units, step), :] = slab[r : r + step]
+
     wk_load.wait()
-    kv_all[me, :, :width] = jnp.dot(scaled, wk_s[...], preferred_element_type=f32)
+    keep_part(jnp.dot(scaled, wk_s[...], preferred_element_type=f32), 0)
     wv_load.wait()
-    kv_all[me, :, width:] = jnp.dot(scaled, wv_s[...], preferred_element_type=f32)
-    send_kv(*kv_args)
+    keep_part(jnp.dot(scaled, wv_s[...], preferred_element_type=f32), heads)
 
     len_load.wait()
     lam_load.wait()
@@ -122,14 +131,30 @@
     col = lax.broadcasted_iota(jnp.int32, (2 * heads, cols), 1)
     row = lax.broadcasted_iota(jnp.int32, (2 * heads, cols), 0)
     diagonal = lax.rem(col, heads) == lax.rem(row, heads)
-    local = [len_s[b] - me * span for b in range(seqs)]
-    for b in range(seqs):
-        bias_s[b] = jnp.where(diagonal & (col < local[b] * heads), f32(0.0), f32(-jnp.inf))
+    for b in range(seqs):
+        before = (len_s[b] - me * span) * heads
+        bias_s[b] = jnp.where(diagonal & (col < before), f32(0.0), f32(-jnp.inf))
     lane = lax.broadcasted_iota(jnp.int32, (2 * heads, vdim), 1)
     half = lax.broadcasted_iota(jnp.int32, (2 * heads, vdim), 0) // heads
     own_map = (lane // head_width) == half
 
-    wait_kv(*q_args, False)
+    wait_kv(*q_args, False, range(1, 2))
+
+    def part_copy(o, sent):
+        peer = lax.rem(me + o, n)
+        slot = me if sent else peer
+        return pltpu.make_async_remote_copy(
+            src_ref=kv_part.at[peer], dst_ref=kv_in.at[slot],
+            send_sem=part_send.at[o], recv_sem=part_recv.at[slot],
+            device_id={"kv": peer}, device_id_type=MESH,
+        )
+
+    for o in range(1, n):
+        part_copy(o, True).start()
+    wait_kv(*q_args, False, range(2, n))
+    for b in range(seqs):
+        k_loads[b].wait()
+        v_loads[b].wait()
     total = q_all[0]
     for s in range(1, n):
         total = total + q_all[s]
@@ -141,70 +166,86 @@
     def doubled(rows):
         return jnp.concatenate([rows, rows], axis=0)
 
-    queries, scores = [], []
-    for b in range(seqs):
-        q_b = jnp.where(own_map, doubled(q_rows[b]), f32(0.0))
-        queries.append(q_b)
-    for b in range(seqs):
-        k_loads[b].wait()
-        scores.append(
+    queries = [
+        jnp.where(own_map, doubled(q_rows[b]), f32(0.0)) * head_width**-0.5 for b in range(seqs)
+    ]
+    stats = jnp.zeros(stat_all.shape[1:], f32)
+    stat_lane = lax.broadcasted_iota(jnp.int32, stats.shape, 1)
+    for b in range(seqs):
+        score = (
             lax.dot_general(
-                (queries[b] * head_width**-0.5).astype(jnp.bfloat16), kc_s[b],
+                queries[b].astype(jnp.bfloat16), kc_s[b],
                 (((1,), (1,)), ((), ())), preferred_element_type=f32,
             )
             + bias_s[b]
         )
-        bias_s[b] = scores[b]
-
-    wait_kv(*kv_args, False)
-    total = kv_all[0]
-    for s in range(1, n):
-        total = total + kv_all[s]
-    fresh = (total * inv).astype(jnp.bfloat16)
-    nk_ref[...] = fresh[:, :width]
-    nv_ref[...] = fresh[:, width:]
-    fresh = fresh.astype(f32)
-    for h in range(heads):
-        k_rows[:, h, :] = fresh[:, h * vdim : (h + 1) * vdim]
-        v_rows[:, h, :] = fresh[:, width + h * vdim : width + (h + 1) * vdim]
-
-    stats = jnp.zeros((2 * heads, stat_all.shape[2]), f32)
-    stat_lane = lax.broadcasted_iota(jnp.int32, stats.shape, 1)
-    for b in range(seqs):
-        new_score = jnp.sum(queries[b] * doubled(k_rows[b]), axis=-1, keepdims=True)
-        here = (local[b] >= 0) & (local[b] < span)
-        new_score = jnp.where(here, new_score * head_width**-0.5, f32(-jnp.inf))
-        score = bias_s[b]
-        peak = jnp.maximum(jnp.max(score, axis=-1, keepdims=True), new_score)
-        peak = jnp.maximum(peak, f32(-1e30))
+        peak = jnp.maximum(jnp.max(score, axis=-1, keepdims=True), f32(-1e30))
         weights = jnp.exp(score - peak)
-        new_weight = jnp.exp(new_score - peak)
-        block_sum = jnp.sum(weights, axis=-1, keepdims=True) + new_weight
-        v_loads[b].wait()
+        block_sum = jnp.sum(weights, axis=-1, keepdims=True)
         acc = jnp.dot(weights.astype(jnp.bfloat16), vc_s[b], preferred_element_type=f32)
-        acc_all[me, b] = acc + new_weight.astype(jnp.bfloat16).astype(f32) * doubled(v_rows[b])
+        acc_all[me, b] = acc.astype(acc_all.dtype)
         send_kv(*acc_args[b])
-        stats = jnp.where(stat_lane == b, peak, stats)
-        stats = jnp.where(stat_lane == seqs + b, block_sum, stats)
-    stat_all[me] = stats
-    send_kv(*stat_args)
+        for j in range(2):
+            rows = slice(j * heads, (j + 1) * heads)
+            stats = jnp.where(stat_lane == 2 * b + j, peak[rows], stats)
+            stats = jnp.where(stat_lane == 2 * (seqs + b) + j, block_sum[rows], stats)
+        if b == seqs - 1:
+            stat_all[me] = stats
+            send_kv(*stat_args)
+        if b == (seqs - 1) // 2:
+            share = kv_part[me]
+            for o in range(1, n):
+                part_copy(o, False).wait_recv()
+                share = share + kv_in[lax.rem(me + o, n)]
+            unit = me * units + lax.broadcasted_iota(jnp.int32, (units, 1), 0)
+            seq = lax.rem(unit, seqs)
+            scale = jnp.zeros((units, 1), f32)
+            for c in range(seqs):
+                scale = jnp.where(seq == c, inv[c : c + 1], scale)
+            kv_out[me] = (share * scale).astype(jnp.bfloat16)
+            send_kv(*kv_args)
 
     h_row = lax.broadcasted_iota(jnp.int32, (heads, 1), 0)
     lam = jnp.zeros((heads, 1), f32)
     for h in range(heads):
         lam = jnp.where(h_row == h, lam_s[h], lam)
 
+    wait_kv(*kv_args, False)
+    for s in range(n):
+        fresh_s[pl.ds(s * units, units), :] = kv_out[s].astype(f32)
+    for h in range(heads):
+        place = slice(h * vdim, (h + 1) * vdim)
+        nk_ref[:, place] = fresh_s[pl.ds(h * seqs, seqs), :].astype(jnp.bfloat16)
+        nv_ref[:, place] = fresh_s[pl.ds((heads + h) * seqs, seqs), :].astype(jnp.bfloat16)
+
+    new_scores, new_values = [], []
+    for b in range(seqs):
+        new_key = doubled(fresh_s[pl.ds(b, heads, stride=seqs), :])
+        new_values.append(doubled(fresh_s[pl.ds(heads * seqs + b, heads, stride=seqs), :]))
+        new_scores.append(jnp.sum(queries[b] * new_key, axis=-1, keepdims=True))
+
     wait_kv(*stat_args, False)
-    for b in range(seqs):
-        peaks = [stat_all[s][:, b : b + 1] for s in range(n)]
-        sums = [stat_all[s][:, seqs + b : seqs + b + 1] for s in range(n)]
-        top = functools.reduce(jnp.maximum, peaks)
+
+    def stat(s, i):
+        return jnp.concatenate([stat_all[s][:, 2 * i + j : 2 * i + j + 1] for j in range(2)], axis=0)
+
+    weighted = []
+    for b in range(seqs):
+        peaks = [stat(s, b) for s in range(n)]
+        top = functools.reduce(jnp.maximum, peaks, new_scores[b])
         factors = [jnp.exp(p - top) for p in peaks]
-        whole_sum = sum(l * f for l, f in zip(sums, factors))
+        new_factor = jnp.exp(new_scores[b] - top)
+        whole_sum = new_factor
+        for s in range(n):
+            whole_sum = whole_sum + stat(s, seqs + b) * factors[s]
+        weighted.append((factors, new_factor, whole_sum))
+    for b in range(seqs):
         wait_kv(*acc_args[b], False)
-        summed = acc_all[0, b] * factors[0]
-        for s in range(1, n):
-            summed = summed + acc_all[s, b] * factors[s]
+    for b in range(seqs):
+        factors, new_factor, whole_sum = weighted[b]
+        summed = new_values[b] * new_factor
+        for s in range(n):
+            summed = summed + acc_all[s, b].astype(f32) * factors[s]
         maps = summed / whole_sum
         mixed = maps[:heads] - lam * maps[heads:]
         normed = (
@@ -225,6 +266,8 @@
             device_id={"tp": lax.rem(side + o, ntp)}, device_id_type=MESH,
         ).start()
     wait_kv(*q_args, True)
+    for o in range(1, n):
+        part_copy(o, True).wait_send()
     wait_kv(*kv_args, True)
     wait_kv(*stat_args, True)
     for b in range(seqs):
@@ -242,6 +285,15 @@
     for s in range(1, ntp):
         result = result + tp_all[s].astype(f32)
     out_ref[...] = result.astype(jnp.bfloat16)
+
+
+def store(a_ref, b_ref, c_ref, a_out, b_out, c_out, sem):
+    pairs = ((a_ref, a_out), (b_ref, b_out), (c_ref, c_out))
+    copies = [pltpu.make_async_copy(src, dst, sem.at[i]) for i, (src, dst) in enumerate(pairs)]
+    for copy in copies:
+        copy.start()
+    for copy in copies:
+        copy.wait()
 
 
 def per_device(
@@ -259,14 +311,12 @@
     vmem, dma = pltpu.VMEM, pltpu.SemaphoreType.DMA
     keys = key_cache.reshape(seqs, span * heads, vdim)
     values = value_cache.reshape(seqs, span * heads, vdim)
+    units = 2 * heads * seqs // n
     body = functools.partial(kernel, n, ntp, features * n, vdim // 2)
-    return pl.pallas_call(
+    shapes = ((seqs, columns), (seqs, width), (seqs, width))
+    parts = pl.pallas_call(
         body,
-        out_shape=(
-            jax.ShapeDtypeStruct((seqs, columns), bf16),
-            jax.ShapeDtypeStruct((seqs, width), bf16),
-            jax.ShapeDtypeStruct((seqs, width), bf16),
-        ),
+        out_shape=tuple(vmem(shape, bf16) for shape in shapes),
         in_specs=[pl.BlockSpec(memory_space=HBM)] * 11,
         out_specs=(pl.BlockSpec(memory_space=pltpu.VMEM),) * 3,
         scratch_shapes=[
@@ -282,17 +332,18 @@
             pltpu.SMEM((heads,), f32),
             vmem((1, vdim), f32),
             vmem((n, seqs, width + 128), f32),
-            vmem((n, seqs, 2 * width), f32),
-            vmem((n, seqs, 2 * heads, vdim), f32),
-            vmem((n, 2 * heads, 128), f32),
+            vmem((n, units, vdim), f32),
+            vmem((n, units, vdim), f32),
+            vmem((n, units, vdim), bf16),
+            vmem((n, seqs, 2 * heads, vdim), bf16),
+            vmem((n, heads, 128), f32),
             vmem((ntp, seqs, columns), bf16),
             vmem((seqs, 2 * heads, span * heads), f32),
             vmem((seqs, heads, vdim), f32),
-            vmem((seqs, heads, vdim), f32),
-            vmem((seqs, heads, vdim), f32),
+            vmem((2 * heads * seqs, vdim), f32),
             vmem((seqs, heads, vdim), f32),
             dma((9,)), dma((seqs,)), dma((seqs,)),
-            dma((n,)), dma((n,)), dma((n,)), dma((n,)),
+            dma((n,)), dma((n,)), dma((n,)), dma((n,)), dma((n,)), dma((n,)),
             dma((n, seqs)), dma((n, seqs)), dma((n,)), dma((n,)),
             dma((ntp,)), dma((ntp,)),
         ],
@@ -303,6 +354,14 @@
         tokens, norm_gain.reshape(1, -1), w_query, w_key, w_value, w_output,
         keys, values, lengths, lam, head_gain.reshape(1, -1),
     )
+    return pl.pallas_call(
+        store,
+        out_shape=tuple(jax.ShapeDtypeStruct(shape, bf16) for shape in shapes),
+        in_specs=[pl.BlockSpec(memory_space=pltpu.VMEM)] * 3,
+        out_specs=(pl.BlockSpec(memory_space=HBM),) * 3,
+        scratch_shapes=[dma((3,))],
+        compiler_params=pltpu.CompilerParams(vmem_limit_bytes=1024 * 1024),
+    )(*parts)
 
 
 def solution(mesh):

time: 25.1 us -> 20.8 us (0.83)
  local copies, waits for them, and re-layouts: 3.87 us -> 0 us
    unnamed x3 -> x0, local copies, waits for them, and re-layouts: 3.87 us -> none
    pallas_call x1 -> x2, Pallas kernels: 20.2 us -> 20 us  [the longest x1 19.3 us: per_device(): pl.pallas_call(body, out_shape=tuple((vmem(shape, bf16) for shape in shap...]
where the time goes in v2:
time: 20.8 us; the launch traced here: 20.6 us
  Pallas kernels  20 us (96%)
  between operations  0.64 us (3%)
    pallas_call x1, Pallas kernels, per_device(): pl.pallas_call(body, out_shape=tuple((vmem(shape, bf16) for shape in shap...  19.3 us
    pallas_call x1, Pallas kernels, per_device(): pl.pallas_call(store, out_shape=tuple((jax.ShapeDtypeStruct(shape, bf16)...  0.64 us

profile of v2, /device:TPU:0, one launch (start us, length us, event | category | flops | bytes accessed | tf_op | source)
XLA Modules:
  0.0 20.6 jit_solution(8019534579890708088)
XLA Ops:
  0.6 19.3 %shard_map.130 = (bf16[4,512]{1,0:T(4,128)(2,1)S(1)}, bf16[4,1024]{1,0:T(4,128)(2,1)S(1)}, bf16[4,1024]{1,0:T(4,128)(2,1)S(1)}) custom-call(bf16[4,512]{1,0:T(4,128)(2,1)} %x_hbm.1, f32[1,512]{1,0:T(1,128)} %bitcast.6, bf16[512,1024]{1,0:T(8,128)(2,1)} %wq_hbm.1, bf16[512,1024]{1,0:T(8,128)(2,1)} %wk_hbm.1, bf16[512,1024]{1,0:T(8,128)(2,1)} %wv_hbm.1, ...), custom_call_target="tpu_custom_call" | custom-call | tf_op jit(solution)/shard_map/pallas_call | solution.py:317
  20.0 0.6 %shard_map.131 = (bf16[4,512]{1,0:T(4,128)(2,1)}, bf16[4,1024]{1,0:T(4,128)(2,1)}, bf16[4,1024]{1,0:T(4,128)(2,1)}) custom-call(bf16[4,512]{1,0:T(4,128)(2,1)S(1)} %get-tuple-element.6.a_ref, bf16[4,1024]{1,0:T(4,128)(2,1)S(1)} %get-tuple-element.7.b_ref, bf16[4,1024]{1,0:T(4,128)(2,1)S(1)} %get-tuple-element.8.c_ref), custom_call_target="tpu_custom_call" | custom-call | tf_op jit(solution)/shard_map/pallas_call | solution.py:357

commit v3 on v2

--- a/solution.py
+++ b/solution.py
@@ -17,9 +17,9 @@
     x_hbm, g_hbm, wq_hbm, wk_hbm, wv_hbm, wo_hbm, kc_hbm, vc_hbm, len_hbm, lam_hbm, hg_hbm,
     out_ref, nk_ref, nv_ref,
     x_s, g_s, wq_s, wk_s, wv_s, wo_s, kc_s, vc_s, len_s, lam_s, hg_s,
-    q_all, kv_part, kv_in, kv_out, acc_all, stat_all, tp_all, bias_s, q_rows, fresh_s, head_rows,
+    q_all, kv_all, acc_all, stat_all, tp_all, bias_s, q_rows, fresh_s, head_rows,
     load_sem, k_sem, v_sem,
-    q_send, q_recv, part_send, part_recv, kv_send, kv_recv, acc_send, acc_recv, stat_send, stat_recv, tp_send, tp_recv,
+    q_send, q_recv, kv_send, kv_recv, acc_send, acc_recv, stat_send, stat_recv, tp_send, tp_recv,
 ):
     me = lax.axis_index("kv")
     side = lax.axis_index("tp")
@@ -39,11 +39,6 @@
     x_load = load(x_hbm, x_s, 0)
     g_load = load(g_hbm, g_s, 1)
     wq_load = load(wq_hbm, wq_s, 2)
-    len_load = load(len_hbm, len_s, 3)
-    wk_load = load(wk_hbm, wk_s, 4)
-    wv_load = load(wv_hbm, wv_s, 5)
-    lam_load = load(lam_hbm, lam_s, 6)
-    hg_load = load(hg_hbm, hg_s, 7)
 
     barrier = pltpu.get_barrier_semaphore()
     for o in range(1, n):
@@ -54,13 +49,19 @@
         pl.semaphore_signal(
             barrier, inc=1, device_id={"tp": lax.rem(side + o, ntp)}, device_id_type=MESH
         )
+
+    def far_peer(o):
+        k = o - 1
+        down = n - 1 - k - lax.div(me + k, n - 1)
+        up = k + lax.div(k - me + n, n)
+        return down + lax.div(2 * me, n) * (up - down)
 
     def send_kv(buf, at, send, recv):
         for o in range(1, n):
             pltpu.make_async_remote_copy(
                 src_ref=buf.at[at(me)], dst_ref=buf.at[at(me)],
                 send_sem=send(o), recv_sem=recv(me),
-                device_id={"kv": lax.rem(me + o, n)}, device_id_type=MESH,
+                device_id={"kv": far_peer(o)}, device_id_type=MESH,
             ).start()
 
     def wait_kv(buf, at, send, recv, sent, offsets=range(1, n)):
@@ -82,6 +83,11 @@
     squares = jnp.sum(xf * xf, axis=-1, keepdims=True)
     scaled = (xf * g_s[...]).astype(jnp.bfloat16)
     wq_load.wait()
+    wk_load = load(wk_hbm, wk_s, 4)
+    wv_load = load(wv_hbm, wv_s, 5)
+    len_load = load(len_hbm, len_s, 3)
+    lam_load = load(lam_hbm, lam_s, 6)
+    hg_load = load(hg_hbm, hg_s, 7)
     k_loads, v_loads = [], []
     for b in range(seqs):
         copy = pltpu.make_async_copy(kc_hbm.at[b], kc_s.at[b], k_sem.at[b])
@@ -98,7 +104,7 @@
     pl.semaphore_wait(barrier, n - 1 + ntp - 1)
     whole = lambda s: s
     q_args = (q_all, whole, lambda o: q_send.at[o], lambda s: q_recv.at[s])
-    kv_args = (kv_out, whole, lambda o: kv_send.at[o], lambda s: kv_recv.at[s])
+    kv_args = (kv_all, whole, lambda o: kv_send.at[o], lambda s: kv_recv.at[s])
     stat_args = (stat_all, whole, lambda o: stat_send.at[o], lambda s: stat_recv.at[s])
     acc_args = [
         (
@@ -110,20 +116,10 @@
         for b in range(seqs)
     ]
     send_kv(*q_args)
-    units = kv_part.shape[1]
-
-    def keep_part(part, first):
-        for h in range(heads):
-            slab = part[:, h * vdim : (h + 1) * vdim]
-            at = (first + h) * seqs
-            step = min(seqs, units)
-            for r in range(0, seqs, step):
-                kv_part[(at + r) // units, pl.ds((at + r) % units, step), :] = slab[r : r + step]
-
     wk_load.wait()
-    keep_part(jnp.dot(scaled, wk_s[...], preferred_element_type=f32), 0)
+    kv_all[me, :, :width] = jnp.dot(scaled, wk_s[...], preferred_element_type=f32)
     wv_load.wait()
-    keep_part(jnp.dot(scaled, wv_s[...], preferred_element_type=f32), heads)
+    kv_all[me, :, width:] = jnp.dot(scaled, wv_s[...], preferred_element_type=f32)
 
     len_load.wait()
     lam_load.wait()
@@ -140,17 +136,7 @@
 
     wait_kv(*q_args, False, range(1, 2))
 
-    def part_copy(o, sent):
-        peer = lax.rem(me + o, n)
-        slot = me if sent else peer
-        return pltpu.make_async_remote_copy(
-            src_ref=kv_part.at[peer], dst_ref=kv_in.at[slot],
-            send_sem=part_send.at[o], recv_sem=part_recv.at[slot],
-            device_id={"kv": peer}, device_id_type=MESH,
-        )
-
-    for o in range(1, n):
-        part_copy(o, True).start()
+    send_kv(*kv_args)
     wait_kv(*q_args, False, range(2, n))
     for b in range(seqs):
         k_loads[b].wait()
@@ -171,6 +157,7 @@
     ]
     stats = jnp.zeros(stat_all.shape[1:], f32)
     stat_lane = lax.broadcasted_iota(jnp.int32, stats.shape, 1)
+    rounded = []
     for b in range(seqs):
         score = (
             lax.dot_general(
@@ -182,28 +169,17 @@
         peak = jnp.maximum(jnp.max(score, axis=-1, keepdims=True), f32(-1e30))
         weights = jnp.exp(score - peak)
         block_sum = jnp.sum(weights, axis=-1, keepdims=True)
-        acc = jnp.dot(weights.astype(jnp.bfloat16), vc_s[b], preferred_element_type=f32)
-        acc_all[me, b] = acc.astype(acc_all.dtype)
-        send_kv(*acc_args[b])
+        rounded.append(weights.astype(jnp.bfloat16))
         for j in range(2):
             rows = slice(j * heads, (j + 1) * heads)
             stats = jnp.where(stat_lane == 2 * b + j, peak[rows], stats)
             stats = jnp.where(stat_lane == 2 * (seqs + b) + j, block_sum[rows], stats)
-        if b == seqs - 1:
-            stat_all[me] = stats
-            send_kv(*stat_args)
-        if b == (seqs - 1) // 2:
-            share = kv_part[me]
-            for o in range(1, n):
-                part_copy(o, False).wait_recv()
-                share = share + kv_in[lax.rem(me + o, n)]
-            unit = me * units + lax.broadcasted_iota(jnp.int32, (units, 1), 0)
-            seq = lax.rem(unit, seqs)
-            scale = jnp.zeros((units, 1), f32)
-            for c in range(seqs):
-                scale = jnp.where(seq == c, inv[c : c + 1], scale)
-            kv_out[me] = (share * scale).astype(jnp.bfloat16)
-            send_kv(*kv_args)
+    stat_all[me] = stats
+    send_kv(*stat_args)
+    for b in range(seqs):
+        acc = jnp.dot(rounded[b], vc_s[b], preferred_element_type=f32)
+        acc_all[me, b] = acc.astype(acc_all.dtype)
+        send_kv(*acc_args[b])
 
     h_row = lax.broadcasted_iota(jnp.int32, (heads, 1), 0)
     lam = jnp.zeros((heads, 1), f32)
@@ -211,17 +187,20 @@
         lam = jnp.where(h_row == h, lam_s[h], lam)
 
     wait_kv(*kv_args, False)
-    for s in range(n):
-        fresh_s[pl.ds(s * units, units), :] = kv_out[s].astype(f32)
-    for h in range(heads):
-        place = slice(h * vdim, (h + 1) * vdim)
-        nk_ref[:, place] = fresh_s[pl.ds(h * seqs, seqs), :].astype(jnp.bfloat16)
-        nv_ref[:, place] = fresh_s[pl.ds((heads + h) * seqs, seqs), :].astype(jnp.bfloat16)
+    total = kv_all[0]
+    for s in range(1, n):
+        total = total + kv_all[s]
+    fresh = (total * inv).astype(jnp.bfloat16)
+    nk_ref[...] = fresh[:, :width]
+    nv_ref[...] = fresh[:, width:]
+    fresh = fresh.astype(f32)
+    for i in range(2 * heads):
+        fresh_s[:, i, :] = fresh[:, i * vdim : (i + 1) * vdim]
 
     new_scores, new_values = [], []
     for b in range(seqs):
-        new_key = doubled(fresh_s[pl.ds(b, heads, stride=seqs), :])
-        new_values.append(doubled(fresh_s[pl.ds(heads * seqs + b, heads, stride=seqs), :]))
+        new_key = doubled(fresh_s[b, :heads])
+        new_values.append(doubled(fresh_s[b, heads:]))
         new_scores.append(jnp.sum(queries[b] * new_key, axis=-1, keepdims=True))
 
     wait_kv(*stat_args, False)
@@ -266,8 +245,6 @@
             device_id={"tp": lax.rem(side + o, ntp)}, device_id_type=MESH,
         ).start()
     wait_kv(*q_args, True)
-    for o in range(1, n):
-        part_copy(o, True).wait_send()
     wait_kv(*kv_args, True)
     wait_kv(*stat_args, True)
     for b in range(seqs):
@@ -311,7 +288,6 @@
     vmem, dma = pltpu.VMEM, pltpu.SemaphoreType.DMA
     keys = key_cache.reshape(seqs, span * heads, vdim)
     values = value_cache.reshape(seqs, span * heads, vdim)
-    units = 2 * heads * seqs // n
     body = functools.partial(kernel, n, ntp, features * n, vdim // 2)
     shapes = ((seqs, columns), (seqs, width), (seqs, width))
     parts = pl.pallas_call(
@@ -332,18 +308,16 @@
             pltpu.SMEM((heads,), f32),
             vmem((1, vdim), f32),
             vmem((n, seqs, width + 128), f32),
-            vmem((n, units, vdim), f32),
-            vmem((n, units, vdim), f32),
-            vmem((n, units, vdim), bf16),
+            vmem((n, seqs, 2 * width), f32),
             vmem((n, seqs, 2 * heads, vdim), bf16),
             vmem((n, heads, 128), f32),
             vmem((ntp, seqs, columns), bf16),
             vmem((seqs, 2 * heads, span * heads), f32),
             vmem((seqs, heads, vdim), f32),
-            vmem((2 * heads * seqs, vdim), f32),
+            vmem((seqs, 2 * heads, vdim), f32),
             vmem((seqs, heads, vdim), f32),
             dma((9,)), dma((seqs,)), dma((seqs,)),
-            dma((n,)), dma((n,)), dma((n,)), dma((n,)), dma((n,)), dma((n,)),
+            dma((n,)), dma((n,)), dma((n,)), dma((n,)),
             dma((n, seqs)), dma((n, seqs)), dma((n,)), dma((n,)),
             dma((ntp,)), dma((ntp,)),
         ],

time: 20.8 us -> 18.4 us (0.88)
  Pallas kernels: 20 us -> 17.6 us
    pallas_call x1, Pallas kernels: 19.3 us -> 16.9 us  [per_device(): pl.pallas_call(body, out_shape=tuple((vmem(shape, bf16) for shape in shap...]
where the time goes in v3:
time: 18.4 us; the launch traced here: 18.2 us
  Pallas kernels  17.6 us (96%)
  between operations  0.64 us (3%)
    pallas_call x1, Pallas kernels, per_device(): pl.pallas_call(body, out_shape=tuple((vmem(shape, bf16) for shape in shap...  16.9 us
    pallas_call x1, Pallas kernels, per_device(): pl.pallas_call(store, out_shape=tuple((jax.ShapeDtypeStruct(shape, bf16)...  0.64 us

profile of v3, /device:TPU:0, one launch (start us, length us, event | category | flops | bytes accessed | tf_op | source)
XLA Modules:
  0.0 18.2 jit_solution(8033950115995496431)
XLA Ops:
  0.6 16.9 %shard_map.130 = (bf16[4,512]{1,0:T(4,128)(2,1)S(1)}, bf16[4,1024]{1,0:T(4,128)(2,1)S(1)}, bf16[4,1024]{1,0:T(4,128)(2,1)S(1)}) custom-call(bf16[4,512]{1,0:T(4,128)(2,1)} %x_hbm.1, f32[1,512]{1,0:T(1,128)} %bitcast.6, bf16[512,1024]{1,0:T(8,128)(2,1)} %wq_hbm.1, bf16[512,1024]{1,0:T(8,128)(2,1)} %wk_hbm.1, bf16[512,1024]{1,0:T(8,128)(2,1)} %wv_hbm.1, ...), custom_call_target="tpu_custom_call" | custom-call | tf_op jit(solution)/shard_map/pallas_call | solution.py:293
  17.6 0.6 %shard_map.131 = (bf16[4,512]{1,0:T(4,128)(2,1)}, bf16[4,1024]{1,0:T(4,128)(2,1)}, bf16[4,1024]{1,0:T(4,128)(2,1)}) custom-call(bf16[4,512]{1,0:T(4,128)(2,1)S(1)} %get-tuple-element.6.a_ref, bf16[4,1024]{1,0:T(4,128)(2,1)S(1)} %get-tuple-element.7.b_ref, bf16[4,1024]{1,0:T(4,128)(2,1)S(1)} %get-tuple-element.8.c_ref), custom_call_target="tpu_custom_call" | custom-call | tf_op jit(solution)/shard_map/pallas_call | solution.py:331

commit v4 on v3

--- a/solution.py
+++ b/solution.py
@@ -40,21 +40,21 @@
     g_load = load(g_hbm, g_s, 1)
     wq_load = load(wq_hbm, wq_s, 2)
 
-    barrier = pltpu.get_barrier_semaphore()
-    for o in range(1, n):
-        pl.semaphore_signal(
-            barrier, inc=1, device_id={"kv": lax.rem(me + o, n)}, device_id_type=MESH
-        )
-    for o in range(1, ntp):
-        pl.semaphore_signal(
-            barrier, inc=1, device_id={"tp": lax.rem(side + o, ntp)}, device_id_type=MESH
-        )
-
     def far_peer(o):
         k = o - 1
         down = n - 1 - k - lax.div(me + k, n - 1)
         up = k + lax.div(k - me + n, n)
         return down + lax.div(2 * me, n) * (up - down)
+
+    barrier = pltpu.get_barrier_semaphore()
+    for o in range(1, n):
+        pl.semaphore_signal(
+            barrier, inc=1, device_id={"kv": far_peer(o)}, device_id_type=MESH
+        )
+    for o in range(1, ntp):
+        pl.semaphore_signal(
+            barrier, inc=1, device_id={"tp": lax.rem(side + o, ntp)}, device_id_type=MESH
+        )
 
     def send_kv(buf, at, send, recv):
         for o in range(1, n):
@@ -106,15 +106,7 @@
     q_args = (q_all, whole, lambda o: q_send.at[o], lambda s: q_recv.at[s])
     kv_args = (kv_all, whole, lambda o: kv_send.at[o], lambda s: kv_recv.at[s])
     stat_args = (stat_all, whole, lambda o: stat_send.at[o], lambda s: stat_recv.at[s])
-    acc_args = [
-        (
-            acc_all,
-            lambda s, b=b: (s, b),
-            lambda o, b=b: acc_send.at[o, b],
-            lambda s, b=b: acc_recv.at[s, b],
-        )
-        for b in range(seqs)
-    ]
+    acc_args = (acc_all, whole, lambda o: acc_send.at[o], lambda s: acc_recv.at[s])
     send_kv(*q_args)
     wk_load.wait()
     kv_all[me, :, :width] = jnp.dot(scaled, wk_s[...], preferred_element_type=f32)
@@ -140,7 +132,6 @@
     wait_kv(*q_args, False, range(2, n))
     for b in range(seqs):
         k_loads[b].wait()
-        v_loads[b].wait()
     total = q_all[0]
     for s in range(1, n):
         total = total + q_all[s]
@@ -177,9 +168,12 @@
     stat_all[me] = stats
     send_kv(*stat_args)
     for b in range(seqs):
+        v_loads[b].wait()
+    for b in range(seqs):
         acc = jnp.dot(rounded[b], vc_s[b], preferred_element_type=f32)
         acc_all[me, b] = acc.astype(acc_all.dtype)
-        send_kv(*acc_args[b])
+        if b == seqs - 1:
+            send_kv(*acc_args)
 
     h_row = lax.broadcasted_iota(jnp.int32, (heads, 1), 0)
     lam = jnp.zeros((heads, 1), f32)
@@ -219,7 +213,8 @@
             whole_sum = whole_sum + stat(s, seqs + b) * factors[s]
         weighted.append((factors, new_factor, whole_sum))
     for b in range(seqs):
-        wait_kv(*acc_args[b], False)
+        if b == 0:
+            wait_kv(*acc_args, False)
     for b in range(seqs):
         factors, new_factor, whole_sum = weighted[b]
         summed = new_values[b] * new_factor
@@ -248,7 +243,8 @@
     wait_kv(*kv_args, True)
     wait_kv(*stat_args, True)
     for b in range(seqs):
-        wait_kv(*acc_args[b], True)
+        if b == 0:
+            wait_kv(*acc_args, True)
     for o in range(1, ntp):
         src = lax.rem(side + o, ntp)
         copy = pltpu.make_async_remote_copy(
@@ -318,7 +314,7 @@
             vmem((seqs, heads, vdim), f32),
             dma((9,)), dma((seqs,)), dma((seqs,)),
             dma((n,)), dma((n,)), dma((n,)), dma((n,)),
-            dma((n, seqs)), dma((n, seqs)), dma((n,)), dma((n,)),
+            dma((n,)), dma((n,)), dma((n,)), dma((n,)),
             dma((ntp,)), dma((ntp,)),
         ],
         compiler_params=pltpu.CompilerParams(

time: 18.4 us -> 17.8 us (0.967)
  Pallas kernels: 17.6 us -> 17 us
    pallas_call x1, Pallas kernels: 16.9 us -> 16.4 us  [per_device(): pl.pallas_call(body, out_shape=tuple((vmem(shape, bf16) for shape in shap...]
where the time goes in v4:
time: 17.8 us; the launch traced here: 17.6 us
  Pallas kernels  17 us (96%)
  between operations  0.64 us (4%)
    pallas_call x1, Pallas kernels, per_device(): pl.pallas_call(body, out_shape=tuple((vmem(shape, bf16) for shape in shap...  16.4 us
    pallas_call x1, Pallas kernels, per_device(): pl.pallas_call(store, out_shape=tuple((jax.ShapeDtypeStruct(shape, bf16)...  0.64 us

profile of v4, /device:TPU:0, one launch (start us, length us, event | category | flops | bytes accessed | tf_op | source)
XLA Modules:
  0.0 17.6 jit_solution(11741851928203351939)
XLA Ops:
  0.6 16.4 %shard_map.130 = (bf16[4,512]{1,0:T(4,128)(2,1)S(1)}, bf16[4,1024]{1,0:T(4,128)(2,1)S(1)}, bf16[4,1024]{1,0:T(4,128)(2,1)S(1)}) custom-call(bf16[4,512]{1,0:T(4,128)(2,1)} %x_hbm.1, f32[1,512]{1,0:T(1,128)} %bitcast.6, bf16[512,1024]{1,0:T(8,128)(2,1)} %wq_hbm.1, bf16[512,1024]{1,0:T(8,128)(2,1)} %wk_hbm.1, bf16[512,1024]{1,0:T(8,128)(2,1)} %wv_hbm.1, ...), custom_call_target="tpu_custom_call" | custom-call | tf_op jit(solution)/shard_map/pallas_call | solution.py:289
  17.0 0.6 %shard_map.131 = (bf16[4,512]{1,0:T(4,128)(2,1)}, bf16[4,1024]{1,0:T(4,128)(2,1)}, bf16[4,1024]{1,0:T(4,128)(2,1)}) custom-call(bf16[4,512]{1,0:T(4,128)(2,1)S(1)} %get-tuple-element.6.a_ref, bf16[4,1024]{1,0:T(4,128)(2,1)S(1)} %get-tuple-element.7.b_ref, bf16[4,1024]{1,0:T(4,128)(2,1)S(1)} %get-tuple-element.8.c_ref), custom_call_target="tpu_custom_call" | custom-call | tf_op jit(solution)/shard_map/pallas_call | solution.py:327
